TPU v7x, 32 devices: a whole 2x2x4 slice. The times are simulated.
32 devices in a mesh: sp: 8 (over z, y), tp: 4 (over x, core).
Axes of the slice: x: 2, y: 2, z: 4, core: 2. Of those that a mesh axis runs over, the one named last changes fastest.
Arguments:
- latent: bfloat16 [2048, 2048], P('sp'), may hold values from -6 to 6
- context: bfloat16 [512, 2048], P('sp'), may hold values from -6 to 6
- condition: float32 [2048], P('sp'), may hold values from -6 to 6
- ctx_condition: float32 [2048], P('sp'), may hold values from -6 to 6
- shift_weight: bfloat16 [2048, 2048], P('sp', 'tp'), may hold values from -0.125 to 0.125
- scale_weight: bfloat16 [2048, 2048], P('sp', 'tp'), may hold values from -0.125 to 0.125
- gate_weight: bfloat16 [2048, 2048], P('sp', 'tp'), may hold values from -0.125 to 0.125
- norm_gain: float32 [2048], replicated, may hold values from 0.1 to 1.9
- query_weight: bfloat16 [2048, 1024], P(None, 'tp'), may hold values from -0.125 to 0.125
- key_weight: bfloat16 [2048, 1024], P(None, 'tp'), may hold values from -0.125 to 0.125
- value_weight: bfloat16 [2048, 1024], P(None, 'tp'), may hold values from -0.125 to 0.125
- query_gain: float32 [64], replicated, may hold values from 0.6 to 6.5
- key_gain: float32 [64], replicated, may hold values from 0.6 to 6.5
- offset_bias: float32 [16, 15, 31], P('tp'), may hold values from 1 to 3
- out_weight: bfloat16 [1024, 2048], P('tp'), may hold values from -0.75 to 0.75
Outputs:
- mixed_rows: bfloat16 [2048, 2048], P('sp')
All inputs are finite; a program needn't handle non-finite values.
Results may differ from a plain program's by a relative error of at most 0.01405.
The roundings to bfloat16 on the way count: a program that leaves them out, or rounds other values in their place, can miss the bound.
Values may be sent and summed in bfloat16 or wider, within the bound.
A program may use at most 64 MiB of HBM per device.

v0:
```python
import jax
import jax.numpy as jnp
from jax import lax
from jax.sharding import PartitionSpec as P

HEAD_DIM = 64
GRID_W = 64
WIN_ROWS = 8
WIN_COLS = 16


EPS = 1e-06


def extended(x, sides, width):
    for axis, dim in sides:
        count, length = (lax.axis_size(axis), x.shape[dim])
        up = [(i, (i + 1) % count) for i in range(count - 1)]
        down = [(j, i) for i, j in up]
        last = lax.slice_in_dim(x, length - width, length, axis=dim)
        initial = lax.slice_in_dim(x, 0, width, axis=dim)
        before = lax.ppermute(last, axis, up)
        after = lax.ppermute(initial, axis, down)
        x = jnp.concatenate([before, x, after], axis=dim)
    return x


def modulate(rows_in, norm_gain, shift_vec, scale_vec):
    values = rows_in.astype(jnp.float32)
    normed = values * lax.rsqrt(jnp.mean(values * values, axis=-1, keepdims=True) + EPS)
    return (normed * norm_gain * (1.0 + scale_vec) + shift_vec).astype(jnp.bfloat16)


def head_norm(projected, head_gain):
    row_count = projected.shape[0]
    split_heads = projected.reshape(row_count, -1, head_gain.shape[0])
    normed = split_heads * lax.rsqrt(
        jnp.mean(split_heads * split_heads, axis=-1, keepdims=True) + EPS
    )
    return (normed * head_gain).astype(jnp.bfloat16).reshape(row_count, -1)


def per_device(
    latent,
    context,
    condition,
    ctx_condition,
    shift_weight,
    scale_weight,
    gate_weight,
    norm_gain,
    query_weight,
    key_weight,
    value_weight,
    query_gain,
    key_gain,
    offset_bias,
    out_weight,
):
    activations = jax.nn.silu(jnp.stack([condition, ctx_condition])).astype(jnp.bfloat16)
    part_shift = jnp.dot(activations, shift_weight, preferred_element_type=jnp.float32)
    part_scale = jnp.dot(activations, scale_weight, preferred_element_type=jnp.float32)
    part_gate = jnp.dot(activations[:1], gate_weight, preferred_element_type=jnp.float32)
    block_cols = shift_weight.shape[1]
    first_col = lax.axis_index("tp") * block_cols

    def spread(piece_part):
        padded_vec = jnp.zeros((piece_part.shape[0], block_cols * lax.axis_size("tp")), jnp.float32)
        return lax.dynamic_update_slice_in_dim(padded_vec, piece_part, first_col, 1)

    shift_vec, scale_vec, gate_vec = lax.psum(
        (spread(part_shift), spread(part_scale), spread(part_gate)), ("sp", "tp")
    )
    hidden = modulate(latent, norm_gain, shift_vec[0], scale_vec[0])
    queries = head_norm(
        jnp.dot(hidden, query_weight, preferred_element_type=jnp.float32), query_gain
    )
    keys_lat = head_norm(jnp.dot(hidden, key_weight, preferred_element_type=jnp.float32), key_gain)
    values_lat = jnp.dot(hidden, value_weight, preferred_element_type=jnp.float32).astype(
        jnp.bfloat16
    )
    ctx_hidden = modulate(
        lax.all_gather(context, "sp", axis=0, tiled=True), norm_gain, shift_vec[1], scale_vec[1]
    )
    ctx_keys = head_norm(
        jnp.dot(ctx_hidden, key_weight, preferred_element_type=jnp.float32), key_gain
    )
    ctx_values = jnp.dot(ctx_hidden, value_weight, preferred_element_type=jnp.float32).astype(
        jnp.bfloat16
    )
    ctx_pairs = jnp.concatenate([ctx_keys, ctx_values], axis=1)
    col_width = keys_lat.shape[1]
    heads_dev = col_width // HEAD_DIM
    local_rows = keys_lat.shape[0] // GRID_W
    halo_rows = WIN_ROWS // 2
    window_keys = WIN_ROWS * GRID_W
    key_value = jnp.concatenate([keys_lat, values_lat], axis=1).reshape(
        local_rows, GRID_W, 2 * col_width
    )
    padded = extended(key_value, (("sp", 0),), halo_rows)
    first_row = lax.axis_index("sp") * local_rows
    total_rows = local_rows * lax.axis_size("sp")
    global_rows = first_row + jnp.arange(local_rows, dtype=jnp.int32)
    band_start = jnp.clip(global_rows - halo_rows, 0, total_rows - WIN_ROWS)
    band_global = band_start[:, None] + jnp.arange(WIN_ROWS, dtype=jnp.int32)[None, :]
    banded = jnp.take(padded, band_global - first_row + halo_rows, axis=0)
    key_band = banded[..., :col_width].reshape(local_rows, window_keys, heads_dev, HEAD_DIM)
    value_band = banded[..., col_width:].reshape(local_rows, window_keys, heads_dev, HEAD_DIM)
    row_steps = band_global - global_rows[:, None] + WIN_ROWS - 1
    row_hot = (
        row_steps[:, :, None] == jnp.arange(2 * WIN_ROWS - 1, dtype=jnp.int32)[None, None, :]
    ).astype(jnp.float32)
    column_ids = jnp.arange(GRID_W, dtype=jnp.int32)
    col_steps = (
        jnp.clip(column_ids[None, :] - column_ids[:, None], 1 - WIN_COLS, WIN_COLS - 1)
        + WIN_COLS
        - 1
    )
    col_hot = (
        col_steps[:, :, None] == jnp.arange(2 * WIN_COLS - 1, dtype=jnp.int32)[None, None, :]
    ).astype(jnp.float32)
    col_start = jnp.clip(column_ids - WIN_COLS // 2, 0, GRID_W - WIN_COLS)
    col_open = (column_ids[None, :] >= col_start[:, None]) & (
        column_ids[None, :] < col_start[:, None] + WIN_COLS
    )
    col_table = jnp.einsum("hab,qkb->haqk", offset_bias, col_hot, precision=lax.Precision.HIGHEST)
    col_table = jnp.where(col_open[None, None, :, :], col_table, -jnp.inf)
    offset_terms = jnp.einsum(
        "rja,haqk->hrqjk",
        row_hot,
        jnp.where(col_open[None, None], col_table, 0.0),
        precision=lax.Precision.HIGHEST,
    )
    offset_terms = jnp.where(col_open[None, None, :, None, :], offset_terms, -jnp.inf)
    offset_terms = offset_terms.reshape(heads_dev, local_rows, GRID_W, window_keys)
    score_scale = HEAD_DIM ** (-0.5)
    q_grid = queries.reshape(local_rows, GRID_W, heads_dev, HEAD_DIM)
    scores = (
        jnp.einsum("rqhd,rnhd->hrqn", q_grid, key_band, preferred_element_type=jnp.float32)
        * score_scale
        + offset_terms
    )
    ctx_count = ctx_pairs.shape[0]
    ctx_keys_all = ctx_pairs[:, :col_width].reshape(ctx_count, heads_dev, HEAD_DIM)
    ctx_values_all = ctx_pairs[:, col_width:].reshape(ctx_count, heads_dev, HEAD_DIM)
    ctx_scores = (
        jnp.einsum("rqhd,nhd->hrqn", q_grid, ctx_keys_all, preferred_element_type=jnp.float32)
        * score_scale
    )
    row_max = jnp.maximum(jnp.max(scores, axis=3), jnp.max(ctx_scores, axis=3))
    local_exp = jnp.exp(scores - row_max[..., None])
    ctx_exp = jnp.exp(ctx_scores - row_max[..., None])
    denominator = jnp.sum(local_exp, axis=3) + jnp.sum(ctx_exp, axis=3)
    local_weights = (local_exp / denominator[..., None]).astype(jnp.bfloat16)
    ctx_weights = (ctx_exp / denominator[..., None]).astype(jnp.bfloat16)
    combined = jnp.einsum(
        "hrqn,rnhd->rqhd", local_weights, value_band, preferred_element_type=jnp.float32
    ) + jnp.einsum(
        "hrqn,nhd->rqhd", ctx_weights, ctx_values_all, preferred_element_type=jnp.float32
    )
    attended = combined.astype(jnp.bfloat16).reshape(local_rows * GRID_W, col_width)
    partial_value = jnp.dot(attended, out_weight, preferred_element_type=jnp.float32)
    branch = lax.psum(partial_value.astype(jnp.bfloat16), "tp").astype(jnp.float32)
    return (latent.astype(jnp.float32) + gate_vec[0] * branch).astype(jnp.bfloat16)


def solution(mesh):
    in_specs = (
        P("sp", None),
        P("sp", None),
        P("sp"),
        P("sp"),
        P("sp", "tp"),
        P("sp", "tp"),
        P("sp", "tp"),
        P(),
        P(None, "tp"),
        P(None, "tp"),
        P(None, "tp"),
        P(),
        P(),
        P("tp", None, None),
        P("tp", None),
    )
    out_specs = P("sp", None)
    return jax.shard_map(
        per_device, mesh=mesh, in_specs=in_specs, out_specs=out_specs, check_vma=False
    )
```

profile of v0, /device:TPU:1, one launch (start us, length us, event | category | flops | bytes accessed | tf_op | source)
XLA Modules:
  0.0 170.5 jit_solution(17375178177945889908)
XLA Ops:
  6.5 1.6 fusion.5
  8.1 0.7 fusion.53
  8.9 1.1 fusion.54
  10.0 1.1 convolution_dynamic-update-slice_fusion.1
  11.1 1.1 convolution_dynamic-update-slice_fusion
  12.4 41.0 %all-reduce = (f32[2,2048]{1,0:T(2,128)S(1)}, f32[2,2048]{1,0:T(2,128)S(1)}, f32[2048]{0:T(1024)S(1)}) all-reduce(f32[2,2048]{1,0:T(2,128)S(1)} %convolution_dynamic-update-slice_fusion, f32[2,2048]{1,0:T(2,128)S(1)} %convolution_dynamic-update-slice_fusion.1, ...), channel_id=1, replica_groups=mesh['sp'=8,'tp'=4] {'sp','tp'}, use_global_device_ids=true, to_apply=%region_3.4 | all-reduce | flops 10240 | bytes 81920 | tf_op jit(solution)/shard_map/psum | solution.py:71
  53.4 2.2 %fusion.64 = (f32[256,256]{1,0:T(8,128)S(1)}, f32[256,256]{1,0:T(8,128)S(1)}) fusion(bf16[2048,256]{1,0:T(8,128)(2,1)} %param.24, bf16[256,2048]{1,0:T(8,128)(2,1)} %param.15, f32[2048]{0:T(1024)S(1)} %bitcast.100, f32[2048]{0:T(1024)S(1)} %bitcast.97, f32[2048]{0:T(1024)} %param.22, f32[256]{0:T(256)S(1)} %add_rsqrt_fusion.4), kind=kOutput, calls=%fused_computation.101 | convolution fusion | flops 271646720 | bytes 2647040 | tf_op jit(solution)/shard_map/dot_general | solution.py:78
  56.1 1.8 %convolution_convert_fusion.2 = bf16[256,256]{1,0:T(8,128)(2,1)S(1)} fusion(bf16[2048,256]{1,0:T(8,128)(2,1)} %param.25, bf16[256,2048]{1,0:T(8,128)(2,1)S(1)} %copy-done.2, f32[2048]{0:T(1024)S(1)} %bitcast.101, f32[2048]{0:T(1024)S(1)} %bitcast.98, f32[2048]{0:T(1024)S(1)} %copy-done.10, f32[256]{0:T(256)S(1)} %add_rsqrt_fusion.4), kind=kOutput, calls=%fused_computation.40 | convolution fusion | flops 271646720 | bytes 2253824 | tf_op jit(solution)/shard_map/dot_general | solution.py:79
  58.0 3.0 %collective-permute-start = (bf16[4,64,512]{2,1,0:T(8,128)(2,1)S(1)}, bf16[4,64,512]{2,1,0:T(8,128)(2,1)S(1)}, u32[]{:S(2)}, u32[]{:S(2)}) collective-permute-start(bf16[4,64,512]{2,1,0:T(8,128)(2,1)S(1)} %pad_maximum_fusion.1), channel_id=1, source_target_pairs={{0,4},{4,8},{8,12},{12,16},{16,20},{20,24},{24,28},{1,5},{5,9},{9,... | collective-permute-start | bytes 786440 | tf_op jit(solution)/shard_map/ppermute | solution.py:22
  61.0 1.3 collective-permute-start.1
  62.7 2.0 %bitcast_reduce_fusion = (f32[256,4]{0,1:T(4,128)S(1)}, f32[256,256]{0,1:T(8,128)S(1)}) fusion(bf16[2048,256]{1,0:T(8,128)(2,1)} %param.23, bf16[256,2048]{1,0:T(8,128)(2,1)S(1)} %copy-done.2, f32[2048]{0:T(1024)S(1)} %bitcast.102, f32[2048]{0:T(1024)S(1)} %bitcast.99, f32[2048]{0:T(1024)S(1)} %copy-done.10, f32[256]{0:T(256)S(1)} %add_rsqrt_fusion.4), kind=kOutput, calls=%fused_computation.59 | convolution fusion | flops 271711232 | bytes 2388992 | tf_op jit(solution)/shard_map/dot_general | solution.py:76
  64.8 1.0 fusion.36
  65.8 3.9 %select_bitcast_fusion = f32[4,4,64,8,64]{4,3,1,2,0:T(8,128)} fusion(f32[64,64,4,15]{1,3,0,2:T(8,128)S(1)} %fusion.36, pred[64,64]{1,0:T(8,128)(4,1)S(1)} %fusion.49, s32[4,8]{1,0:T(4,128)S(1)} %subtract_add_fusion), kind=kOutput, calls=%fused_computation.8 | convolution fusion | flops 95388128 | bytes 3084416 | tf_op jit(solution)/shard_map/rja,haqk->hrqjk/dot_general | solution.py:128
  69.9 1.0 copy.33
  71.0 5.1 %reshape.331 = f32[4,4,64,512]{3,1,2,0:T(4,128)} reshape(f32[4,4,64,8,64]{4,3,1,2,0:T(8,128)} %select_bitcast_fusion) | data formatting | bytes 4194304 | tf_op jit(solution)/shard_map/reshape | solution.py:135
  76.3 2.0 %gather_fusion = bf16[32,64,512]{2,1,0:T(8,128)(2,1)} fusion(bf16[12,64,512]{2,1,0:T(8,128)(2,1)S(1)} %pad_maximum_fusion, s32[1024]{0:T(1024)S(1)} %pad_clamp_fusion), kind=kCustom, calls=%fused_computation | custom fusion | bytes 4194432 | tf_op jit(solution)/shard_map/jit(_take)/gather | solution.py:106
  78.4 1.9 %broadcast_select_fusion = bf16[4,8,64,512]{3,2,1,0:T(8,128)(2,1)S(1)} fusion(bf16[4,8,64,512]{3,2,1,0:T(8,128)(2,1)} %bitcast.83, pred[4,8]{1,0:T(4,128)(4,1)S(1)} %compare_and_fusion), kind=kLoop, calls=%fused_computation.31 | loop fusion | flops 1048576 | bytes 4194336 | tf_op jit(solution)/shard_map/jit(_take)/select_n | solution.py:106
  80.5 1.8 %reshape.330 = bf16[4,512,4,64]{3,2,1,0:T(4,128)(2,1)} reshape(bf16[4,8,64,256]{3,2,1,0:T(8,128)(2,1)S(1)} %get-tuple-element.11) | data formatting | bytes 2097152 | tf_op jit(solution)/shard_map/reshape | solution.py:107
  82.3 1.9 %reshape.329 = bf16[4,512,4,64]{3,2,1,0:T(4,128)(2,1)} reshape(bf16[4,8,64,256]{3,2,1,0:T(8,128)(2,1)S(1)} %get-tuple-element.10) | data formatting | bytes 2097152 | tf_op jit(solution)/shard_map/reshape | solution.py:108
  84.2 3.7 %fusion.65 = (f32[4,4,64]{2,1,0:T(4,128)S(1)}, f32[4,4,64,512]{3,2,1,0:T(8,128)S(1)}) fusion(f32[4,4,64,512]{3,1,2,0:T(4,128)} %reshape.331, bf16[4,512,4,64]{3,2,1,0:T(4,128)(2,1)} %reshape.330, f32[4,64,4,64]{3,1,0,2:T(8,128)} %copy.33, f32[64]{0:T(128)S(1)} %copy-done.7, f32[4,64,4]{1,0,2:T(4,128)S(1)} %rsqrt.46), kind=kOutput, calls=%fused_computation.102 | convolution fusion | flops 68877312 | bytes 5513472 | tf_op jit(solution)/shard_map/rqhd,rnhd->hrqn/dot_general | solution.py:139
  87.8 24.8 %all-gather.2.cloned.1.call-done = bf16[512,2048]{1,0:T(8,128)(2,1)} async-done(((bf16[64,2048]{1,0:T(8,128)(2,1)}), bf16[512,2048]{1,0:T(8,128)(2,1)}) %all-gather.2.cloned.1.call-update) | async-done | bytes 2097168 | tf_op jit(solution)/shard_map/all_gather | solution.py:83
  112.6 2.2 %fusion = f32[512]{0:T(512)S(1)} fusion(bf16[512,2048]{1,0:T(8,128)(2,1)} %all-gather.2.cloned.1.call-done), kind=kLoop, calls=%fused_computation.3 | loop fusion | flops 3145216 | bytes 2099200 | tf_op jit(solution)/shard_map/reduce_sum | solution.py:30
  114.9 2.5 %multiply_reduce_fusion.1 = (f32[512,4]{0,1:T(4,128)S(1)}, f32[512,256]{0,1:T(8,128)S(1)}) fusion(bf16[2048,256]{1,0:T(8,128)(2,1)} %param.24, bf16[512,2048]{1,0:T(8,128)(2,1)S(1)} %copy-done.4, f32[2048]{0:T(1024)S(1)} %bitcast.95, f32[2048]{0:T(1024)S(1)} %bitcast.93, f32[2048]{0:T(1024)S(1)} %copy-done.10, f32[512]{0:T(512)S(1)} %add_rsqrt_fusion.3), kind=kOutput, calls=%fused_computation.53 | convolution fusion | flops 543422464 | bytes 3704832 | tf_op jit(solution)/shard_map/dot_general | solution.py:86
  117.4 0.6 multiply_reduce_fusion
  118.0 0.8 fusion.19
  118.8 0.8 divide_convert_fusion.1
  120.0 1.2 convolution_convert_fusion.1
  121.2 0.6 convolution_bitcast_fusion
  121.8 0.9 fusion.28
  123.1 1.4 convolution_convert_fusion
  124.6 36.5 %all-reduce.3.cloned.1.call-done = bf16[256,2048]{1,0:T(8,128)(2,1)} async-done(((bf16[256,2048]{1,0:T(8,128)(2,1)}), bf16[256,2048]{1,0:T(8,128)(2,1)}) %all-reduce.3.cloned.1.call-update) | async-done | bytes 1048592 | tf_op jit(solution)/shard_map/psum | solution.py:163
  161.1 2.6 %fusion.10 = bf16[256,2048]{1,0:T(8,128)(2,1)} fusion(bf16[256,2048]{1,0:T(8,128)(2,1)S(1)} %copy-done.3, bf16[256,2048]{1,0:T(8,128)(2,1)} %all-reduce.3.cloned.1.call-done, f32[2048]{0:T(1024)S(1)} %get-tuple-element.9), kind=kLoop, calls=%fused_computation.18 | loop fusion | flops 2621440 | bytes 3153920 | tf_op jit(solution)/shard_map/convert_element_type | solution.py:164
  (64 shorter events, 2.8 us)
Async XLA Ops:
  6.5 116.6 %copy-start = (bf16[256,2048]{1,0:T(8,128)(2,1)S(1)}, bf16[256,2048]{1,0:T(8,128)(2,1)}, u32[]{:S(2)}) copy-start(bf16[256,2048]{1,0:T(8,128)(2,1)} %param.29) | copy-start | bytes 3145732
  6.5 106.1 %all-gather.2.cloned.1.call-start = ((), (), s32[]{:S(2)}) async-start(), calls=%async_computation | async-start | bytes 2359296 | tf_op jit(solution)/shard_map/all_gather | solution.py:83
  53.4 2.6 %copy-start.8 = (f32[64]{0:T(128)S(1)}, f32[64]{0:T(128)}, u32[]{:S(2)}) copy-start(f32[64]{0:T(128)} %param.27) | copy-start | bytes 772
  53.4 2.7 %copy-start.2 = (bf16[256,2048]{1,0:T(8,128)(2,1)S(1)}, bf16[256,2048]{1,0:T(8,128)(2,1)}, u32[]{:S(2)}) copy-start(bf16[256,2048]{1,0:T(8,128)(2,1)} %param.15) | copy-start | bytes 3145732
  53.4 2.7 %copy-start.10 = (f32[2048]{0:T(1024)S(1)}, f32[2048]{0:T(1024)}, u32[]{:S(2)}) copy-start(f32[2048]{0:T(1024)} %param.22) | copy-start | bytes 24580
  58.0 18.2 %collective-permute-start = (bf16[4,64,512]{2,1,0:T(8,128)(2,1)S(1)}, bf16[4,64,512]{2,1,0:T(8,128)(2,1)S(1)}, u32[]{:S(2)}, u32[]{:S(2)}) collective-permute-start(bf16[4,64,512]{2,1,0:T(8,128)(2,1)S(1)} %pad_maximum_fusion.1), channel_id=1, source_target_pairs={{0,4},{4,8},{8,12},{12,16},{16,20},{20,24},{24,28},{1,5},{5,9},{9,... | collective-permute-start | bytes 786440 | tf_op jit(solution)/shard_map/ppermute | solution.py:22
  61.0 15.2 %collective-permute-start.1 = (bf16[4,64,512]{2,1,0:T(8,128)(2,1)S(1)}, bf16[4,64,512]{2,1,0:T(8,128)(2,1)S(1)}, u32[]{:S(2)}, u32[]{:S(2)}) collective-permute-start(bf16[4,64,512]{2,1,0:T(8,128)(2,1)S(1)} %pad_maximum_fusion.1), channel_id=1, source_target_pairs={{4,0},{8,4},{12,8},{16,12},{20,16},{24,20},{28,24},{5,1},{9,5},{13... | collective-permute-start | bytes 786440 | tf_op jit(solution)/shard_map/ppermute | solution.py:23
  62.3 2.5 %copy-start.6 = (f32[4,15,31]{2,0,1:T(4,128)S(1)}, f32[4,15,31]{2,0,1:T(4,128)}, u32[]{:S(2)}) copy-start(f32[4,15,31]{2,0,1:T(4,128)} %param.28) | copy-start | bytes 22324
  62.3 98.8 %all-reduce.3.cloned.1.call-start = ((), (), s32[]{:S(2)}) async-start(), calls=%async_computation.1 | async-start | bytes 2097152 | tf_op jit(solution)/shard_map/psum | solution.py:163
  82.3 1.9 %copy-start.7 = (f32[64]{0:T(128)S(1)}, f32[64]{0:T(128)}, u32[]{:S(2)}) copy-start(f32[64]{0:T(128)} %param.26) | copy-start | bytes 772
  112.6 2.2 %copy-start.4 = (bf16[512,2048]{1,0:T(8,128)(2,1)S(1)}, bf16[512,2048]{1,0:T(8,128)(2,1)}, u32[]{:S(2)}) copy-start(bf16[512,2048]{1,0:T(8,128)(2,1)} %all-gather.2.cloned.1.call-done) | copy-start | bytes 6291460
  114.9 2.5 %copy-start.1 = (f32[4,64,4,64]{3,1,0,2:T(8,128)S(1)}, f32[4,64,4,64]{3,1,0,2:T(8,128)}, u32[]{:S(2)}) copy-start(f32[4,64,4,64]{3,1,0,2:T(8,128)} %copy.33) | copy-start | bytes 786436
  118.8 1.2 copy-start.9
  120.0 1.8 %copy-start.5 = (bf16[4,512,4,64]{3,2,1,0:T(4,128)(2,1)S(1)}, bf16[4,512,4,64]{3,2,1,0:T(4,128)(2,1)}, u32[]{:S(2)}) copy-start(bf16[4,512,4,64]{3,2,1,0:T(4,128)(2,1)} %reshape.329) | copy-start | bytes 3145732
  122.7 38.4 %copy-start.3 = (bf16[256,2048]{1,0:T(8,128)(2,1)S(1)}, bf16[256,2048]{1,0:T(8,128)(2,1)}, u32[]{:S(2)}) copy-start(bf16[256,2048]{1,0:T(8,128)(2,1)} %param.15) | copy-start | bytes 3145732
Sparse Core Ops, SparseCore 0:
  62.5 50.1 all-gather.1
  124.7 36.3 all-reduce.2
where the time goes:
time: 172 us; the launch traced here: 171 us
  waiting for transfers between devices  61.4 us (36%)
  blocking collectives  41 us (24%)
  matrix products  25 us (15%)
  local copies, waits for them, and re-layouts  13.9 us (8%)
  between operations  13.7 us (8%)
  other arithmetic  11.2 us (7%)
  starting transfers between devices  4.33 us (3%)
    psum x1, blocking collectives, per_device(): lax.psum((spread(part_shift), spread(part_scale), spread(part_gate)), ('s...  41 us
    psum x1, waiting for transfers between devices, per_device(): lax.psum(partial_value.astype(jnp.bfloat16), 'tp').astype(jnp.float32)  36.5 us
    all_gather x1, waiting for transfers between devices, per_device(): lax.all_gather(context, 'sp', axis=0, tiled=True)  24.8 us
    reshape x1, local copies, waits for them, and re-layouts, per_device(): offset_terms.reshape(heads_dev, local_rows, GRID_W, window_keys)  5.14 us
    dot_general x1, matrix products, per_device(): jnp.einsum('rja,haqk->hrqjk', row_hot, jnp.where(col_open[None, None], co...  3.89 us
    reduce_sum x2, other arithmetic, modulate(): jnp.mean(values * values, axis=-1, keepdims=True) + EPS  3.82 us
    dot_general x1, matrix products, per_device(): jnp.einsum('rqhd,rnhd->hrqn', q_grid, key_band, preferred_element_type=jn...  3.66 us
  transfers between devices with their start and end apart: 4, of which 2 were waited for; matrix products, arithmetic and copies ran while one was open for 15% of the time, Pallas kernels for 0%

commit v1 on v0

--- a/solution.py
+++ b/solution.py
@@ -1,6 +1,10 @@
+import functools
+
 import jax
 import jax.numpy as jnp
 from jax import lax
+from jax.experimental import pallas as pl
+from jax.experimental.pallas import tpu as pltpu
 from jax.sharding import PartitionSpec as P
 
 HEAD_DIM = 64
@@ -40,7 +44,7 @@
     return (normed * head_gain).astype(jnp.bfloat16).reshape(row_count, -1)
 
 
-def per_device(
+def per_device_plain(
     latent,
     context,
     condition,
@@ -164,6 +168,459 @@
     return (latent.astype(jnp.float32) + gate_vec[0] * branch).astype(jnp.bfloat16)
 
 
+MESH = pl.DeviceIdType.MESH
+MASKED = -1e30
+F32 = jnp.float32
+BF16 = jnp.bfloat16
+
+
+def fused_kernel(
+    n_sp,
+    n_tp,
+    latent,
+    context,
+    shift_w,
+    scale_w,
+    gate_w,
+    query_w,
+    key_w,
+    value_w,
+    out_w,
+    cond,
+    ctx_cond,
+    norm_gain,
+    query_gain,
+    key_gain,
+    bias_rows,
+    out,
+    x_in,
+    x_norm,
+    hid,
+    w_mod,
+    w_qkv,
+    w_out,
+    mod_sp,
+    mod_tp,
+    q_s,
+    k_all,
+    v_all,
+    ctx_k,
+    ctx_v,
+    table,
+    att,
+    local_sem,
+    mod_send,
+    mod_recv,
+    modt_send,
+    modt_recv,
+    halo_send,
+    halo_recv,
+    ctx_send,
+    ctx_recv,
+    wo_send,
+    wo_recv,
+    att_send,
+    att_recv,
+):
+    me_s, me_t = lax.axis_index("sp"), lax.axis_index("tp")
+    rows, d = latent.shape
+    c_rows = context.shape[0]
+    width = key_w.shape[1]
+    heads = width // HEAD_DIM
+    block = shift_w.shape[1]
+    l_rows = rows // GRID_W
+    halo = WIN_ROWS // 2
+    win = WIN_ROWS * GRID_W
+    core = lax.rem(me_t, 2)
+    chip = lax.div(me_t, 2)
+    partner = me_t + 1 - 2 * core
+    n_x = n_tp // 2
+
+    def remote(src, dst, send, recv, s, t):
+        return pltpu.make_async_remote_copy(
+            src_ref=src, dst_ref=dst, send_sem=send, recv_sem=recv,
+            device_id=(s, t), device_id_type=MESH,
+        )
+
+    barrier = pltpu.get_barrier_semaphore()
+    for k in range(1, n_sp):
+        pl.semaphore_signal(
+            barrier, inc=1, device_id=(lax.rem(me_s + k, n_sp), me_t), device_id_type=MESH
+        )
+    for k in range(1, n_tp):
+        pl.semaphore_signal(
+            barrier, inc=1, device_id=(me_s, lax.rem(me_t + k, n_tp)), device_id_type=MESH
+        )
+
+    loads = [
+        (shift_w, w_mod.at[0]),
+        (scale_w, w_mod.at[1]),
+        (gate_w, w_mod.at[2]),
+        (context, x_in.at[pl.ds(0, c_rows)]),
+        (latent, x_in.at[pl.ds(c_rows, rows)]),
+        (key_w, w_qkv.at[0]),
+        (value_w, w_qkv.at[1]),
+        (query_w, w_qkv.at[2]),
+        (out_w, w_out.at[me_t]),
+    ]
+    copies = [pltpu.make_async_copy(a, b, local_sem.at[i]) for i, (a, b) in enumerate(loads)]
+    for c in copies:
+        c.start()
+
+    def silu(v):
+        return v / (1.0 + jnp.exp(-v))
+
+    two = (16, cond.shape[1])
+    row_id = lax.broadcasted_iota(jnp.int32, two, 0)
+    act0 = jnp.broadcast_to(silu(cond[...]), two)
+    act1 = jnp.broadcast_to(silu(ctx_cond[...]), two)
+
+    def placed(first, second):
+        picked = jnp.where(row_id == first, act0, 0.0)
+        if second is not None:
+            picked = jnp.where(row_id == second, act1, picked)
+        return picked.astype(BF16)
+
+    part = jnp.zeros((16, block), F32)
+    for i, (first, second) in enumerate(((0, 1), (2, 3), (4, None))):
+        copies[i].wait()
+        part += jnp.dot(placed(first, second), w_mod[i], preferred_element_type=F32)
+    mod_sp[me_s] = part[:8]
+    pl.semaphore_wait(barrier, n_sp + n_tp - 2)
+    sends = []
+    for k in range(1, n_sp):
+        peer = lax.rem(me_s + k, n_sp)
+        c = remote(
+            mod_sp.at[me_s], mod_sp.at[me_s], mod_send.at[k], mod_recv.at[me_s], peer, me_t
+        )
+        c.start()
+        sends.append(c)
+
+    copies[3].wait()
+    copies[4].wait()
+    step = 32
+
+    def norm_rows(i, carry):
+        at = pl.ds(pl.multiple_of(i * step, step), step)
+        v = x_in[at, :].astype(F32)
+        r = lax.rsqrt(jnp.mean(v * v, axis=-1, keepdims=True) + EPS)
+        x_norm[at, :] = v * r * norm_gain[...]
+        return carry
+
+    lax.fori_loop(0, (rows + c_rows) // step, norm_rows, 0)
+
+    pair = 2 * GRID_W
+    q_col = lax.broadcasted_iota(jnp.int32, (GRID_W, pair), 0)
+    k_col = lax.broadcasted_iota(jnp.int32, (GRID_W, pair), 1) % GRID_W
+    col0 = jnp.clip(q_col - WIN_COLS // 2, 0, GRID_W - WIN_COLS)
+    col_open = (k_col >= col0) & (k_col < col0 + WIN_COLS)
+    n_pairs = 2 * WIN_ROWS - 2
+    for h in range(heads):
+        for a in range(n_pairs):
+            line = jnp.broadcast_to(bias_rows[h * n_pairs + a : h * n_pairs + a + 1, :], (GRID_W, pair))
+            rolled = pltpu.roll(line, pair - (WIN_COLS - 1), 1, stride=1, stride_axis=0)
+            table[a, h * GRID_W : (h + 1) * GRID_W, :] = jnp.where(col_open, rolled, MASKED)
+
+    for k in range(1, n_sp):
+        peer = lax.rem(me_s + k, n_sp)
+        remote(
+            mod_sp.at[peer], mod_sp.at[peer], mod_send.at[k], mod_recv.at[peer], peer, me_t
+        ).wait_recv()
+    total = mod_sp[0]
+    for k in range(1, n_sp):
+        total = total + mod_sp[k]
+    mod_tp[me_t] = total
+    for k in range(1, n_tp):
+        peer = lax.rem(me_t + k, n_tp)
+        c = remote(
+            mod_tp.at[me_t], mod_tp.at[me_t], modt_send.at[k], modt_recv.at[me_t], me_s, peer
+        )
+        c.start()
+        sends.append(c)
+
+    def gather_start(buf, send, recv):
+        started = [remote(buf.at[me_t], buf.at[me_t], send.at[0], recv.at[me_t], me_s, partner)]
+        for k in range(1, n_x):
+            far = 2 * lax.rem(chip + k, n_x) + core
+            started.append(
+                remote(buf.at[me_t], buf.at[me_t], send.at[k], recv.at[me_t], me_s, far)
+            )
+        for c in reversed(started):
+            c.start()
+        sends.extend(started)
+
+    def gather_forward(buf, send, recv):
+        for k in range(1, n_x):
+            came = 2 * lax.rem(chip + n_x - k, n_x) + core
+            c = remote(
+                buf.at[came], buf.at[came], send.at[n_x + k], recv.at[came], me_s, partner
+            )
+            c.wait_recv()
+            c.start()
+            sends.append(c)
+
+    def gather_finish(buf, send, recv):
+        remote(
+            buf.at[partner], buf.at[partner], send.at[0], recv.at[partner], me_s, partner
+        ).wait_recv()
+        for k in range(1, n_x):
+            came = 2 * lax.rem(chip + n_x - k, n_x) + 1 - core
+            remote(
+                buf.at[came], buf.at[came], send.at[n_x + k], recv.at[came], me_s, partner
+            ).wait_recv()
+
+    for k in range(1, n_tp):
+        peer = lax.rem(me_t + k, n_tp)
+        remote(
+            mod_tp.at[peer], mod_tp.at[peer], modt_send.at[k], modt_recv.at[peer], me_s, peer
+        ).wait_recv()
+    copies[8].wait()
+    gather_start(w_out, wo_send, wo_recv)
+
+    def vec(r):
+        return jnp.concatenate([mod_tp[j][r : r + 1, :] for j in range(n_tp)], axis=1)
+
+    def modulate_rows(first, count, shift, scale):
+        def body(i, carry):
+            at = pl.ds(pl.multiple_of(first + i * step, step), step)
+            hid[at, :] = (x_norm[at, :] * scale + shift).astype(BF16)
+            return carry
+
+        lax.fori_loop(0, count // step, body, 0)
+
+    modulate_rows(0, c_rows, vec(1), 1.0 + vec(3))
+    modulate_rows(c_rows, rows, vec(0), 1.0 + vec(2))
+
+    head_row = lax.broadcasted_iota(jnp.int32, (width, width), 0) // HEAD_DIM
+    head_col = lax.broadcasted_iota(jnp.int32, (width, width), 1) // HEAD_DIM
+    same_head = (head_row == head_col).astype(F32)
+
+    def head_scale(p, gain):
+        mean = jnp.dot(
+            p * p, same_head, precision=lax.Precision.HIGHEST, preferred_element_type=F32
+        ) * (1.0 / HEAD_DIM)
+        return (p * lax.rsqrt(mean + EPS) * gain[...]).astype(BF16)
+
+    last_s = n_sp - 1
+
+    def share(index, value, block_all, block_ctx):
+        block_ctx[me_s] = value[:c_rows]
+        own = pl.ds(rows, rows)
+        block_all[own, :] = value[c_rows:]
+        up = remote(
+            block_all.at[own], block_all.at[pl.ds(0, rows)],
+            halo_send.at[index, 0], halo_recv.at[index, 0], me_s + 1, me_t,
+        )
+        down = remote(
+            block_all.at[own], block_all.at[pl.ds(2 * rows, rows)],
+            halo_send.at[index, 1], halo_recv.at[index, 1], me_s - 1, me_t,
+        )
+
+        @pl.when(me_s < last_s)
+        def _():
+            up.start()
+
+        @pl.when(me_s > 0)
+        def _():
+            down.start()
+
+        for k in range(1, n_sp):
+            peer = lax.rem(me_s + k, n_sp)
+            c = remote(
+                block_ctx.at[me_s], block_ctx.at[me_s],
+                ctx_send.at[index, k], ctx_recv.at[index, me_s], peer, me_t,
+            )
+            c.start()
+            sends.append(c)
+        return up, down
+
+    copies[5].wait()
+    keys = head_scale(jnp.dot(hid[...], w_qkv[0], preferred_element_type=F32), key_gain)
+    halo_k = share(0, keys, k_all, ctx_k)
+    copies[6].wait()
+    values = jnp.dot(hid[...], w_qkv[1], preferred_element_type=F32).astype(BF16)
+    halo_v = share(1, values, v_all, ctx_v)
+    copies[7].wait()
+    queries = head_scale(
+        jnp.dot(hid[c_rows:, :], w_qkv[2], preferred_element_type=F32), query_gain
+    )
+    q_s[...] = queries * jnp.asarray(HEAD_DIM ** (-0.5), BF16)
+
+    for up, down in (halo_k, halo_v):
+
+        @pl.when(me_s > 0)
+        def _():
+            up.wait_recv()
+
+        @pl.when(me_s < last_s)
+        def _():
+            down.wait_recv()
+
+    for index, block_ctx in enumerate((ctx_k, ctx_v)):
+        for k in range(1, n_sp):
+            peer = lax.rem(me_s + k, n_sp)
+            remote(
+                block_ctx.at[peer], block_ctx.at[peer],
+                ctx_send.at[index, k], ctx_recv.at[index, peer], peer, me_t,
+            ).wait_recv()
+
+    lane_head = lax.broadcasted_iota(jnp.int32, (GRID_W, width), 1) // HEAD_DIM
+    masks = [(lane_head == h).astype(F32) for h in range(heads)]
+    contract_last = (((1,), (1,)), ((), ()))
+    all_ck = ctx_k[...].reshape(n_sp * c_rows, width)
+    all_cv = ctx_v[...].reshape(n_sp * c_rows, width)
+    for i in range(l_rows):
+        start = jnp.where(me_s == 0, halo, jnp.where(me_s == last_s, 0, i))
+        at = pl.ds(pl.multiple_of(start * GRID_W, GRID_W), win)
+        qi = q_s[i * GRID_W : (i + 1) * GRID_W, :].astype(F32)
+        qs = jnp.concatenate([(qi * m).astype(BF16) for m in masks], axis=0)
+        s1 = lax.dot_general(qs, k_all[at, :], contract_last, preferred_element_type=F32)
+        first = start - i + WIN_ROWS - 1 - halo
+        s1 = s1 + jnp.concatenate([table[first + 2 * m] for m in range(WIN_ROWS // 2)], axis=1)
+        s2 = lax.dot_general(qs, all_ck, contract_last, preferred_element_type=F32)
+        top = jnp.maximum(
+            jnp.max(s1, axis=1, keepdims=True), jnp.max(s2, axis=1, keepdims=True)
+        )
+        e1 = jnp.exp(s1 - top)
+        e2 = jnp.exp(s2 - top)
+        inv = 1.0 / (jnp.sum(e1, axis=1, keepdims=True) + jnp.sum(e2, axis=1, keepdims=True))
+        o = jnp.dot((e1 * inv).astype(BF16), v_all[at, :], preferred_element_type=F32)
+        o = o + jnp.dot((e2 * inv).astype(BF16), all_cv, preferred_element_type=F32)
+        picked = o[:GRID_W] * masks[0]
+        for h in range(1, heads):
+            picked = picked + o[h * GRID_W : (h + 1) * GRID_W] * masks[h]
+        att[me_t, i * GRID_W : (i + 1) * GRID_W, :] = picked.astype(BF16)
+
+    gather_forward(w_out, wo_send, wo_recv)
+    gather_start(att, att_send, att_recv)
+    gather_forward(att, att_send, att_recv)
+    gather_finish(w_out, wo_send, wo_recv)
+    gather_finish(att, att_send, att_recv)
+    gate = vec(4)
+    cols = 512
+    for n in range(d // cols):
+        at = slice(n * cols, (n + 1) * cols)
+        branch = jnp.zeros((rows, cols), F32)
+        for j in range(n_tp):
+            branch = branch + jnp.dot(
+                att[j], w_out[j, :, at], preferred_element_type=F32
+            ).astype(BF16).astype(F32)
+        base = x_in[c_rows:, at].astype(F32)
+        out[:, at] = (base + gate[:, at] * branch).astype(BF16)
+
+    for c in sends:
+        c.wait_send()
+    for up, down in (halo_k, halo_v):
+
+        @pl.when(me_s < last_s)
+        def _():
+            up.wait_send()
+
+        @pl.when(me_s > 0)
+        def _():
+            down.wait_send()
+
+
+def per_device(
+    latent,
+    context,
+    condition,
+    ctx_condition,
+    shift_weight,
+    scale_weight,
+    gate_weight,
+    norm_gain,
+    query_weight,
+    key_weight,
+    value_weight,
+    query_gain,
+    key_gain,
+    offset_bias,
+    out_weight,
+):
+    n_sp, n_tp = lax.axis_size("sp"), lax.axis_size("tp")
+    rows, d = latent.shape
+    c_rows = context.shape[0]
+    width = key_weight.shape[1]
+    heads = width // HEAD_DIM
+    block = shift_weight.shape[1]
+    n_pairs = 2 * WIN_ROWS - 2
+    padded = jnp.pad(offset_bias, ((0, 0), (0, 0), (0, GRID_W - offset_bias.shape[2])))
+    bias_rows = jnp.concatenate([padded[:, :-1], padded[:, 1:]], axis=2).reshape(
+        heads * n_pairs, 2 * GRID_W
+    )
+    any_spec = pl.BlockSpec(memory_space=pl.ANY)
+    vmem_spec = pl.BlockSpec(memory_space=pltpu.VMEM)
+    dma = pltpu.SemaphoreType.DMA
+    return pl.pallas_call(
+        functools.partial(fused_kernel, n_sp, n_tp),
+        out_shape=jax.ShapeDtypeStruct((rows, d), BF16),
+        in_specs=[any_spec] * 9 + [vmem_spec] * 6,
+        out_specs=vmem_spec,
+        scratch_shapes=[
+            pltpu.VMEM((rows + c_rows, d), BF16),
+            pltpu.VMEM((rows + c_rows, d), F32),
+            pltpu.VMEM((rows + c_rows, d), BF16),
+            pltpu.VMEM((3, shift_weight.shape[0], block), BF16),
+            pltpu.VMEM((3, d, width), BF16),
+            pltpu.VMEM((n_tp, width, d), BF16),
+            pltpu.VMEM((n_sp, 8, block), F32),
+            pltpu.VMEM((n_tp, 8, block), F32),
+            pltpu.VMEM((rows, width), BF16),
+            pltpu.VMEM((3 * rows, width), BF16),
+            pltpu.VMEM((3 * rows, width), BF16),
+            pltpu.VMEM((n_sp, c_rows, width), BF16),
+            pltpu.VMEM((n_sp, c_rows, width), BF16),
+            pltpu.VMEM((n_pairs, heads * GRID_W, 2 * GRID_W), F32),
+            pltpu.VMEM((n_tp, rows, width), BF16),
+            dma((9,)),
+            dma((n_sp,)),
+            dma((n_sp,)),
+            dma((n_tp,)),
+            dma((n_tp,)),
+            dma((2, 2)),
+            dma((2, 2)),
+            dma((2, n_sp)),
+            dma((2, n_sp)),
+            dma((n_tp,)),
+            dma((n_tp,)),
+            dma((n_tp,)),
+            dma((n_tp,)),
+        ],
+        compiler_params=pltpu.CompilerParams(collective_id=0, has_side_effects=True),
+        name="fused_block",
+    )(
+        latent,
+        context,
+        shift_weight,
+        scale_weight,
+        gate_weight,
+        query_weight,
+        key_weight,
+        value_weight,
+        out_weight,
+        condition.reshape(1, -1),
+        ctx_condition.reshape(1, -1),
+        norm_gain.reshape(1, -1),
+        jnp.tile(query_gain, heads).reshape(1, -1),
+        jnp.tile(key_gain, heads).reshape(1, -1),
+        bias_rows,
+    )
+
+
+def fused_fits(latent, context, condition, query_weight, n_sp, n_tp):
+    rows, c_rows = latent.shape[0] // n_sp, context.shape[0] // n_sp
+    width = query_weight.shape[1] // n_tp
+    return (
+        rows == WIN_ROWS // 2 * GRID_W
+        and c_rows % 32 == 0
+        and condition.shape[0] // n_sp % 128 == 0
+        and width % 128 == 0
+        and n_tp % 2 == 0
+        and n_sp > 1
+    )
+
+
 def solution(mesh):
     in_specs = (
         P("sp", None),
@@ -183,6 +640,13 @@
         P("tp", None),
     )
     out_specs = P("sp", None)
-    return jax.shard_map(
-        per_device, mesh=mesh, in_specs=in_specs, out_specs=out_specs, check_vma=False
-    )
+
+    def step(latent, context, condition, ctx_condition, *rest):
+        n_sp, n_tp = mesh.shape["sp"], mesh.shape["tp"]
+        fits = fused_fits(latent, context, condition, rest[4], n_sp, n_tp)
+        body = per_device if fits else per_device_plain
+        return jax.shard_map(
+            body, mesh=mesh, in_specs=in_specs, out_specs=out_specs, check_vma=False
+        )(latent, context, condition, ctx_condition, *rest)
+
+    return step

time: 172 us -> 52.2 us (0.30)
  waiting for transfers between devices: 61.4 us -> 0 us
  Pallas kernels: 0 us -> 46.1 us
  blocking collectives: 41 us -> 0 us
  matrix products: 25 us -> 0 us
  between operations: 13.7 us -> 0.03 us
  other arithmetic: 11.2 us -> 0.08 us
  local copies, waits for them, and re-layouts: 13.9 us -> 5.73 us
  starting transfers between devices: 4.33 us -> 0 us
    pallas_call x0 -> x1, Pallas kernels: none -> 46.1 us  [per_device(): pl.pallas_call(functools.partial(fused_kernel, n_sp, n_tp), out_shape=jax...]
    psum x1 -> x0, blocking collectives: 41 us -> none  [per_device(): lax.psum((spread(part_shift), spread(part_scale), spread(part_gate)), ('s...]
    psum x1 -> x0, waiting for transfers between devices: 36.5 us -> none  [per_device(): lax.psum(partial_value.astype(jnp.bfloat16), 'tp').astype(jnp.float32)]
    dot_general x15 -> x0, matrix products: 25 us -> none  [the longest x1 3.89 us: per_device(): jnp.einsum('rja,haqk->hrqjk', row_hot, jnp.where(col_open[None, None], co...]
    all_gather x1 -> x0, waiting for transfers between devices: 24.8 us -> none  [per_device(): lax.all_gather(context, 'sp', axis=0, tiled=True)]
    reshape x6 -> x1, local copies, waits for them, and re-layouts: 10.3 us -> 0.61 us  [per_device(): jnp.concatenate([padded[:, :-1], padded[:, 1:]], axis=2)]
    reduce_sum x4 -> x0, other arithmetic: 4.66 us -> none  [the longest x2 3.82 us: modulate(): jnp.mean(values * values, axis=-1, keepdims=True) + EPS]
    ppermute x2 -> x0, starting transfers between devices: 4.28 us -> none  [the longest x1 2.99 us: extended(): before = lax.ppermute(last, axis, up)]
  transfers between devices with their start and end apart: 4 -> 0, of which waited for: 2 -> 0; matrix products, arithmetic and copies ran while one was open for 15% -> 0% of each run, Pallas kernels for 0% -> 0%
where the time goes in v1:
time: 52.2 us; the launch traced here: 51.9 us
  Pallas kernels  46.1 us (88%)
  local copies, waits for them, and re-layouts  5.73 us (11%)
    pallas_call x1, Pallas kernels, per_device(): pl.pallas_call(functools.partial(fused_kernel, n_sp, n_tp), out_shape=jax...  46.1 us
    unnamed x5, local copies, waits for them, and re-layouts  2.96 us

profile of v1, /device:TPU:1, one launch (start us, length us, event | category | flops | bytes accessed | tf_op | source)
XLA Modules:
  0.0 51.9 jit_solution(15365724055923226489)
XLA Ops:
  0.0 0.0 copy-start
  0.0 0.7 %copy-done = f32[64]{0:T(128)S(1)} copy-done((f32[64]{0:T(128)S(1)}, f32[64]{0:T(128)}, u32[]{:S(2)}) %copy-start) | copy-done | bytes 280
  0.7 0.0 copy-start.1
  0.7 0.7 %reshape_tile.6.query_gain = f32[1,256]{1,0:T(1,128)} reshape(f32[4,64]{1,0:T(4,128)S(1)} %tile.4) | data formatting | bytes 2048 | tf_op jit(solution)/shard_map/reshape;tile | solution.py:605
  1.3 0.0 copy-done.1
  1.3 0.7 %reshape_tile.7.key_gain = f32[1,256]{1,0:T(1,128)} reshape(f32[4,64]{1,0:T(4,128)S(1)} %tile.5) | data formatting | bytes 2048 | tf_op jit(solution)/shard_map/reshape;tile | solution.py:606
  2.0 0.8 %pad_slice_fusion.1 = (f32[4,14,64]{2,0,1:T(4,128)S(1)}, f32[4,14,64]{2,0,1:T(4,128)S(1)}) fusion(f32[4,15,31]{2,0,1:T(4,128)} %param.28), kind=kLoop, calls=%fused_computation.2 | loop fusion | bytes 36112 | tf_op jit(solution)/shard_map/slice | solution.py:549
  2.8 0.1 pad_maximum_fusion
  2.9 0.6 %reshape.17.bias_rows = f32[56,128]{1,0:T(8,128)} reshape(f32[4,14,128]{2,1,0:T(8,128)S(1)} %copy.17) | data formatting | bytes 57344 | tf_op jit(solution)/shard_map/reshape | solution.py:549
  3.5 46.1 %fused_block.1 = bf16[256,2048]{1,0:T(8,128)(2,1)} custom-call(bf16[256,2048]{1,0:T(8,128)(2,1)} %latent.1, bf16[64,2048]{1,0:T(8,128)(2,1)} %context.1, bf16[256,512]{1,0:T(8,128)(2,1)} %shift_w.1, bf16[256,512]{1,0:T(8,128)(2,1)} %scale_w.1, bf16[256,512]{1,0:T(8,128)(2,1)} %gate_w.1, bf16[2048,256]{1,0:T(8,128)(2,1)} %query_w.1, bf16[2048,256]{1,0:T(8,128)(2,1)} %key_w.1, ...), custom_call_target="tpu_custom_call" | custom-call | tf_op jit(solution)/shard_map/fused_block/pallas_call | solution.py:555
  49.6 2.3 %copy.19 = bf16[256,2048]{1,0:T(8,128)(2,1)} copy(bf16[256,2048]{1,0:T(8,128)(2,1)} %fused_block.1) | data formatting | bytes 2097152
  (3 shorter events, 0.0 us)
Async XLA Ops:
  0.0 0.7 %copy-start = (f32[64]{0:T(128)S(1)}, f32[64]{0:T(128)}, u32[]{:S(2)}) copy-start(f32[64]{0:T(128)} %param.26) | copy-start | bytes 772
  0.7 0.7 %copy-start.1 = (f32[64]{0:T(128)S(1)}, f32[64]{0:T(128)}, u32[]{:S(2)}) copy-start(f32[64]{0:T(128)} %param.27) | copy-start | bytes 772

commit v2 on v1

--- a/solution.py
+++ b/solution.py
@@ -191,7 +191,7 @@
     norm_gain,
     query_gain,
     key_gain,
-    bias_rows,
+    bias_in,
     out,
     x_in,
     x_norm,
@@ -201,18 +201,28 @@
     w_out,
     mod_sp,
     mod_tp,
-    q_s,
+    q_stage,
+    k_stage,
+    v_stage,
+    ck_stage,
+    cv_stage,
+    q_all,
     k_all,
     v_all,
     ctx_k,
     ctx_v,
+    bias_pad,
+    bias_lines,
     table,
+    att_slab,
     att,
     local_sem,
     mod_send,
     mod_recv,
     modt_send,
     modt_recv,
+    pair_send,
+    pair_recv,
     halo_send,
     halo_recv,
     ctx_send,
@@ -235,6 +245,12 @@
     chip = lax.div(me_t, 2)
     partner = me_t + 1 - 2 * core
     n_x = n_tp // 2
+    side = lax.rem(me_s, 2)
+    slab = lax.div(me_s, 2)
+    mate = me_s + 1 - 2 * side
+    last_slab = n_sp // 2 - 1
+    half = width // 2
+    half_heads = heads // 2
 
     def remote(src, dst, send, recv, s, t):
         return pltpu.make_async_remote_copy(
@@ -315,9 +331,15 @@
     col0 = jnp.clip(q_col - WIN_COLS // 2, 0, GRID_W - WIN_COLS)
     col_open = (k_col >= col0) & (k_col < col0 + WIN_COLS)
     n_pairs = 2 * WIN_ROWS - 2
+    bias_pad[...] = jnp.zeros_like(bias_pad)
     for h in range(heads):
+        bias_pad[h, : 2 * WIN_ROWS - 1, : 2 * WIN_COLS - 1] = bias_in[h]
+    for h in range(half_heads):
+        head = side * half_heads + h
+        upper = pltpu.roll(bias_pad[head, 1 : n_pairs + 1, :], GRID_W, 1)
+        bias_lines[h, :n_pairs, :] = bias_pad[head, :n_pairs, :] + upper
         for a in range(n_pairs):
-            line = jnp.broadcast_to(bias_rows[h * n_pairs + a : h * n_pairs + a + 1, :], (GRID_W, pair))
+            line = jnp.broadcast_to(bias_lines[h, a : a + 1, :], (GRID_W, pair))
             rolled = pltpu.roll(line, pair - (WIN_COLS - 1), 1, stride=1, stride_axis=0)
             table[a, h * GRID_W : (h + 1) * GRID_W, :] = jnp.where(col_open, rolled, MASKED)
 
@@ -399,62 +421,87 @@
         mean = jnp.dot(
             p * p, same_head, precision=lax.Precision.HIGHEST, preferred_element_type=F32
         ) * (1.0 / HEAD_DIM)
-        return (p * lax.rsqrt(mean + EPS) * gain[...]).astype(BF16)
-
-    last_s = n_sp - 1
-
-    def share(index, value, block_all, block_ctx):
-        block_ctx[me_s] = value[:c_rows]
-        own = pl.ds(rows, rows)
-        block_all[own, :] = value[c_rows:]
-        up = remote(
-            block_all.at[own], block_all.at[pl.ds(0, rows)],
-            halo_send.at[index, 0], halo_recv.at[index, 0], me_s + 1, me_t,
-        )
-        down = remote(
-            block_all.at[own], block_all.at[pl.ds(2 * rows, rows)],
-            halo_send.at[index, 1], halo_recv.at[index, 1], me_s - 1, me_t,
-        )
-
-        @pl.when(me_s < last_s)
-        def _():
-            up.start()
-
-        @pl.when(me_s > 0)
-        def _():
-            down.start()
-
+        wide_gain = jnp.concatenate([gain[...]] * heads, axis=1)
+        return (p * lax.rsqrt(mean + EPS) * wide_gain).astype(BF16)
+
+    own = pl.ds(rows + pl.multiple_of(side * rows, rows), rows)
+    other = pl.ds(rows + pl.multiple_of((1 - side) * rows, rows), rows)
+
+    def split(stage, value):
+        for h in range(2):
+            stage[h] = value[:, h * half : (h + 1) * half]
+
+    def trade(index, stage, block_all, at):
+        c = remote(
+            stage.at[1 - side], block_all.at[at], pair_send.at[index], pair_recv.at[index],
+            mate, me_t,
+        )
+        c.start()
+        sends.append(c)
+        return c
+
+    def share_ctx(index, stage, block_ctx):
+        block_ctx[me_s] = stage[side]
         for k in range(1, n_sp):
             peer = lax.rem(me_s + k, n_sp)
             c = remote(
-                block_ctx.at[me_s], block_ctx.at[me_s],
+                stage.at[lax.rem(peer, 2)], block_ctx.at[me_s],
                 ctx_send.at[index, k], ctx_recv.at[index, me_s], peer, me_t,
             )
             c.start()
             sends.append(c)
-        return up, down
+
+    def halo_copies(index, block_all):
+        down = remote(
+            block_all.at[pl.ds(rows, rows)], block_all.at[pl.ds(3 * rows, rows)],
+            halo_send.at[index, 0], halo_recv.at[index, 0], me_s - 2, me_t,
+        )
+        up = remote(
+            block_all.at[pl.ds(2 * rows, rows)], block_all.at[pl.ds(0, rows)],
+            halo_send.at[index, 1], halo_recv.at[index, 1], me_s + 2, me_t,
+        )
+        return down, up
+
+    def halo_start(mine):
+        for index, block_all in enumerate((k_all, v_all)):
+            down, up = halo_copies(index, block_all)
+            is_low = side == 0 if mine else side == 1
+
+            @pl.when(is_low & (slab > 0))
+            def _():
+                down.start()
+
+            @pl.when(jnp.logical_not(is_low) & (slab < last_slab))
+            def _():
+                up.start()
 
     copies[5].wait()
     keys = head_scale(jnp.dot(hid[...], w_qkv[0], preferred_element_type=F32), key_gain)
-    halo_k = share(0, keys, k_all, ctx_k)
+    split(k_stage, keys[c_rows:])
+    k_trade = trade(0, k_stage, k_all, own)
+    split(ck_stage, keys[:c_rows])
+    k_all[own, :] = k_stage[side]
     copies[6].wait()
     values = jnp.dot(hid[...], w_qkv[1], preferred_element_type=F32).astype(BF16)
-    halo_v = share(1, values, v_all, ctx_v)
+    split(v_stage, values[c_rows:])
+    v_trade = trade(1, v_stage, v_all, own)
+    split(cv_stage, values[:c_rows])
+    v_all[own, :] = v_stage[side]
+    halo_start(True)
+    share_ctx(0, ck_stage, ctx_k)
+    share_ctx(1, cv_stage, ctx_v)
     copies[7].wait()
     queries = head_scale(
         jnp.dot(hid[c_rows:, :], w_qkv[2], preferred_element_type=F32), query_gain
-    )
-    q_s[...] = queries * jnp.asarray(HEAD_DIM ** (-0.5), BF16)
-
-    for up, down in (halo_k, halo_v):
-
-        @pl.when(me_s > 0)
-        def _():
-            up.wait_recv()
-
-        @pl.when(me_s < last_s)
-        def _():
-            down.wait_recv()
+    ) * jnp.asarray(HEAD_DIM ** (-0.5), BF16)
+    split(q_stage, queries)
+    q_own = pl.ds(pl.multiple_of(side * rows, rows), rows)
+    q_trade = trade(2, q_stage, q_all, q_own)
+    q_all[q_own, :] = q_stage[side]
+    k_trade.wait_recv()
+    v_trade.wait_recv()
+    halo_start(False)
+    q_trade.wait_recv()
 
     for index, block_ctx in enumerate((ctx_k, ctx_v)):
         for k in range(1, n_sp):
@@ -463,16 +510,34 @@
                 block_ctx.at[peer], block_ctx.at[peer],
                 ctx_send.at[index, k], ctx_recv.at[index, peer], peer, me_t,
             ).wait_recv()
-
-    lane_head = lax.broadcasted_iota(jnp.int32, (GRID_W, width), 1) // HEAD_DIM
-    masks = [(lane_head == h).astype(F32) for h in range(heads)]
+    for index, block_all in enumerate((k_all, v_all)):
+        down, up = halo_copies(index, block_all)
+
+        @pl.when(slab < last_slab)
+        def _():
+            down.wait_recv()
+
+        @pl.when(slab > 0)
+        def _():
+            up.wait_recv()
+
+    lane_head = lax.broadcasted_iota(jnp.int32, (GRID_W, half), 1) // HEAD_DIM
+    masks = [(lane_head == h).astype(F32) for h in range(half_heads)]
     contract_last = (((1,), (1,)), ((), ()))
-    all_ck = ctx_k[...].reshape(n_sp * c_rows, width)
-    all_cv = ctx_v[...].reshape(n_sp * c_rows, width)
-    for i in range(l_rows):
-        start = jnp.where(me_s == 0, halo, jnp.where(me_s == last_s, 0, i))
+    all_ck = ctx_k[...].reshape(n_sp * c_rows, half)
+    all_cv = ctx_v[...].reshape(n_sp * c_rows, half)
+
+    def attend(i):
+        start = jnp.where(
+            slab == 0,
+            jnp.maximum(i, halo),
+            jnp.where(slab == last_slab, jnp.minimum(i, halo), i),
+        )
+        if last_slab == 0:
+            start = jnp.int32(halo)
         at = pl.ds(pl.multiple_of(start * GRID_W, GRID_W), win)
-        qi = q_s[i * GRID_W : (i + 1) * GRID_W, :].astype(F32)
+        row_at = pl.ds(pl.multiple_of(i * GRID_W, GRID_W), GRID_W)
+        qi = q_all[row_at, :].astype(F32)
         qs = jnp.concatenate([(qi * m).astype(BF16) for m in masks], axis=0)
         s1 = lax.dot_general(qs, k_all[at, :], contract_last, preferred_element_type=F32)
         first = start - i + WIN_ROWS - 1 - halo
@@ -487,10 +552,24 @@
         o = jnp.dot((e1 * inv).astype(BF16), v_all[at, :], preferred_element_type=F32)
         o = o + jnp.dot((e2 * inv).astype(BF16), all_cv, preferred_element_type=F32)
         picked = o[:GRID_W] * masks[0]
-        for h in range(1, heads):
+        for h in range(1, half_heads):
             picked = picked + o[h * GRID_W : (h + 1) * GRID_W] * masks[h]
-        att[me_t, i * GRID_W : (i + 1) * GRID_W, :] = picked.astype(BF16)
-
+        return picked.astype(BF16)
+
+    for i in range(l_rows):
+        att_slab[i * GRID_W : (i + 1) * GRID_W, :] = attend((1 - side) * l_rows + i)
+    back = remote(
+        att_slab, att.at[me_t, side], pair_send.at[3], pair_recv.at[3], mate, me_t
+    )
+    back.start()
+    sends.append(back)
+    for i in range(l_rows):
+        att[me_t, side, i * GRID_W : (i + 1) * GRID_W, :] = attend(side * l_rows + i)
+
+    back_in = remote(
+        att_slab, att.at[me_t, 1 - side], pair_send.at[3], pair_recv.at[3], mate, me_t
+    )
+    back_in.wait_recv()
     gather_forward(w_out, wo_send, wo_recv)
     gather_start(att, att_send, att_recv)
     gather_forward(att, att_send, att_recv)
@@ -503,22 +582,25 @@
         branch = jnp.zeros((rows, cols), F32)
         for j in range(n_tp):
             branch = branch + jnp.dot(
-                att[j], w_out[j, :, at], preferred_element_type=F32
+                jnp.concatenate([att[j, 0], att[j, 1]], axis=1),
+                w_out[j, :, at],
+                preferred_element_type=F32,
             ).astype(BF16).astype(F32)
         base = x_in[c_rows:, at].astype(F32)
         out[:, at] = (base + gate[:, at] * branch).astype(BF16)
 
     for c in sends:
         c.wait_send()
-    for up, down in (halo_k, halo_v):
-
-        @pl.when(me_s < last_s)
+    for index, block_all in enumerate((k_all, v_all)):
+        down, up = halo_copies(index, block_all)
+
+        @pl.when(slab > 0)
+        def _():
+            down.wait_send()
+
+        @pl.when(slab < last_slab)
         def _():
             up.wait_send()
-
-        @pl.when(me_s > 0)
-        def _():
-            down.wait_send()
 
 
 def per_device(
@@ -545,10 +627,8 @@
     heads = width // HEAD_DIM
     block = shift_weight.shape[1]
     n_pairs = 2 * WIN_ROWS - 2
-    padded = jnp.pad(offset_bias, ((0, 0), (0, 0), (0, GRID_W - offset_bias.shape[2])))
-    bias_rows = jnp.concatenate([padded[:, :-1], padded[:, 1:]], axis=2).reshape(
-        heads * n_pairs, 2 * GRID_W
-    )
+    half = width // 2
+    half_heads = heads // 2
     any_spec = pl.BlockSpec(memory_space=pl.ANY)
     vmem_spec = pl.BlockSpec(memory_space=pltpu.VMEM)
     dma = pltpu.SemaphoreType.DMA
@@ -566,18 +646,28 @@
             pltpu.VMEM((n_tp, width, d), BF16),
             pltpu.VMEM((n_sp, 8, block), F32),
             pltpu.VMEM((n_tp, 8, block), F32),
-            pltpu.VMEM((rows, width), BF16),
-            pltpu.VMEM((3 * rows, width), BF16),
-            pltpu.VMEM((3 * rows, width), BF16),
-            pltpu.VMEM((n_sp, c_rows, width), BF16),
-            pltpu.VMEM((n_sp, c_rows, width), BF16),
-            pltpu.VMEM((n_pairs, heads * GRID_W, 2 * GRID_W), F32),
-            pltpu.VMEM((n_tp, rows, width), BF16),
+            pltpu.VMEM((2, rows, half), BF16),
+            pltpu.VMEM((2, rows, half), BF16),
+            pltpu.VMEM((2, rows, half), BF16),
+            pltpu.VMEM((2, c_rows, half), BF16),
+            pltpu.VMEM((2, c_rows, half), BF16),
+            pltpu.VMEM((2 * rows, half), BF16),
+            pltpu.VMEM((4 * rows, half), BF16),
+            pltpu.VMEM((4 * rows, half), BF16),
+            pltpu.VMEM((n_sp, c_rows, half), BF16),
+            pltpu.VMEM((n_sp, c_rows, half), BF16),
+            pltpu.VMEM((heads, 2 * WIN_ROWS, 2 * GRID_W), F32),
+            pltpu.VMEM((half_heads, 2 * WIN_ROWS, 2 * GRID_W), F32),
+            pltpu.VMEM((n_pairs, half_heads * GRID_W, 2 * GRID_W), F32),
+            pltpu.VMEM((rows, half), BF16),
+            pltpu.VMEM((n_tp, 2, rows, half), BF16),
             dma((9,)),
             dma((n_sp,)),
             dma((n_sp,)),
             dma((n_tp,)),
             dma((n_tp,)),
+            dma((4,)),
+            dma((4,)),
             dma((2, 2)),
             dma((2, 2)),
             dma((2, n_sp)),
@@ -602,9 +692,9 @@
         condition.reshape(1, -1),
         ctx_condition.reshape(1, -1),
         norm_gain.reshape(1, -1),
-        jnp.tile(query_gain, heads).reshape(1, -1),
-        jnp.tile(key_gain, heads).reshape(1, -1),
-        bias_rows,
+        query_gain.reshape(1, -1),
+        key_gain.reshape(1, -1),
+        offset_bias,
     )
 
 
@@ -615,9 +705,9 @@
         rows == WIN_ROWS // 2 * GRID_W
         and c_rows % 32 == 0
         and condition.shape[0] // n_sp % 128 == 0
-        and width % 128 == 0
+        and width % 256 == 0
         and n_tp % 2 == 0
-        and n_sp > 1
+        and n_sp % 2 == 0
     )
 
 

time: 52.2 us -> 50.1 us (0.960)
  local copies, waits for them, and re-layouts: 5.73 us -> 3.67 us
    another operation x4 -> x0, local copies, waits for them, and re-layouts: 1.32 us -> none  [the longest x2 0.66 us: per_device(): jnp.tile(key_gain, heads).reshape(1, -1)]
    slice x1 -> x0, local copies, waits for them, and re-layouts: 0.84 us -> none  [per_device(): padded[:, :-1]]
    unnamed x5 -> x2, local copies, waits for them, and re-layouts: 2.96 us -> 3.67 us
    reshape x1 -> x0, local copies, waits for them, and re-layouts: 0.61 us -> none  [per_device(): jnp.concatenate([padded[:, :-1], padded[:, 1:]], axis=2)]
where the time goes in v2:
time: 50.1 us; the launch traced here: 49.8 us
  Pallas kernels  46.1 us (92%)
  local copies, waits for them, and re-layouts  3.67 us (7%)
    pallas_call x1, Pallas kernels, per_device(): pl.pallas_call(functools.partial(fused_kernel, n_sp, n_tp), out_shape=jax...  46.1 us
    unnamed x2, local copies, waits for them, and re-layouts  3.67 us

profile of v2, /device:TPU:1, one launch (start us, length us, event | category | flops | bytes accessed | tf_op | source)
XLA Modules:
  0.0 49.8 jit_solution(13685259900911373610)
XLA Ops:
  0.0 1.4 %copy.16.bias_in = f32[4,15,31]{2,1,0:T(8,128)} copy(f32[4,15,31]{2,0,1:T(4,128)} %param.28) | data formatting | bytes 14880 | tf_op args[13]
  1.4 46.1 %fused_block.1 = bf16[256,2048]{1,0:T(8,128)(2,1)} custom-call(bf16[256,2048]{1,0:T(8,128)(2,1)} %latent.1, bf16[64,2048]{1,0:T(8,128)(2,1)} %context.1, bf16[256,512]{1,0:T(8,128)(2,1)} %shift_w.1, bf16[256,512]{1,0:T(8,128)(2,1)} %scale_w.1, bf16[256,512]{1,0:T(8,128)(2,1)} %gate_w.1, bf16[2048,256]{1,0:T(8,128)(2,1)} %query_w.1, bf16[2048,256]{1,0:T(8,128)(2,1)} %key_w.1, ...), custom_call_target="tpu_custom_call" | custom-call | tf_op jit(solution)/shard_map/fused_block/pallas_call | solution.py:635
  47.5 2.3 %copy.18 = bf16[256,2048]{1,0:T(8,128)(2,1)} copy(bf16[256,2048]{1,0:T(8,128)(2,1)} %fused_block.1) | data formatting | bytes 2097152

commit v3 on v2

--- a/solution.py
+++ b/solution.py
@@ -280,7 +280,7 @@
         (out_w, w_out.at[me_t]),
     ]
     copies = [pltpu.make_async_copy(a, b, local_sem.at[i]) for i, (a, b) in enumerate(loads)]
-    for c in copies:
+    for c in copies[:3]:
         c.start()
 
     def silu(v):
@@ -301,6 +301,8 @@
     for i, (first, second) in enumerate(((0, 1), (2, 3), (4, None))):
         copies[i].wait()
         part += jnp.dot(placed(first, second), w_mod[i], preferred_element_type=F32)
+    for c in copies[3:]:
+        c.start()
     mod_sp[me_s] = part[:8]
     pl.semaphore_wait(barrier, n_sp + n_tp - 2)
     sends = []
@@ -311,6 +313,57 @@
         )
         c.start()
         sends.append(c)
+
+    def gather_start(view, sems, source=None):
+        send, recv = sems
+        mine = view(me_t) if source is None else source
+        started = [remote(mine, view(me_t), send(0), recv(me_t), me_s, partner)]
+        for k in range(1, n_x):
+            far = 2 * lax.rem(chip + k, n_x) + core
+            started.append(remote(mine, view(me_t), send(k), recv(me_t), me_s, far))
+        for c in reversed(started):
+            c.start()
+        sends.extend(started)
+
+    def gather_forward(view, sems):
+        send, recv = sems
+        for k in range(1, n_x):
+            came = 2 * lax.rem(chip + n_x - k, n_x) + core
+            c = remote(view(came), view(came), send(n_x + k), recv(came), me_s, partner)
+            c.wait_recv()
+            c.start()
+            sends.append(c)
+
+    def gather_finish(view, sems):
+        send, recv = sems
+        remote(
+            view(partner), view(partner), send(0), recv(partner), me_s, partner
+        ).wait_recv()
+        for k in range(1, n_x):
+            came = 2 * lax.rem(chip + n_x - k, n_x) + 1 - core
+            remote(
+                view(came), view(came), send(n_x + k), recv(came), me_s, partner
+            ).wait_recv()
+
+    early = width // 4
+    wo_rows = (pl.ds(0, early), pl.ds(early, width - early))
+
+    def wo_view(c):
+        return lambda j: w_out.at[j, wo_rows[c]]
+
+    def wo_source(c):
+        return out_w.at[wo_rows[c]]
+
+    def wo_sems(c):
+        return (lambda k: wo_send.at[c, k]), (lambda k: wo_recv.at[c, k])
+
+    def att_view(h):
+        return lambda j: att.at[j, h]
+
+    def att_sems(n):
+        return (lambda k: att_send.at[n, k]), (lambda k: att_recv.at[n, k])
+
+    gather_start(wo_view(0), wo_sems(0), wo_source(0))
 
     copies[3].wait()
     copies[4].wait()
@@ -360,44 +413,13 @@
         c.start()
         sends.append(c)
 
-    def gather_start(buf, send, recv):
-        started = [remote(buf.at[me_t], buf.at[me_t], send.at[0], recv.at[me_t], me_s, partner)]
-        for k in range(1, n_x):
-            far = 2 * lax.rem(chip + k, n_x) + core
-            started.append(
-                remote(buf.at[me_t], buf.at[me_t], send.at[k], recv.at[me_t], me_s, far)
-            )
-        for c in reversed(started):
-            c.start()
-        sends.extend(started)
-
-    def gather_forward(buf, send, recv):
-        for k in range(1, n_x):
-            came = 2 * lax.rem(chip + n_x - k, n_x) + core
-            c = remote(
-                buf.at[came], buf.at[came], send.at[n_x + k], recv.at[came], me_s, partner
-            )
-            c.wait_recv()
-            c.start()
-            sends.append(c)
-
-    def gather_finish(buf, send, recv):
-        remote(
-            buf.at[partner], buf.at[partner], send.at[0], recv.at[partner], me_s, partner
-        ).wait_recv()
-        for k in range(1, n_x):
-            came = 2 * lax.rem(chip + n_x - k, n_x) + 1 - core
-            remote(
-                buf.at[came], buf.at[came], send.at[n_x + k], recv.at[came], me_s, partner
-            ).wait_recv()
+    gather_start(wo_view(1), wo_sems(1), wo_source(1))
 
     for k in range(1, n_tp):
         peer = lax.rem(me_t + k, n_tp)
         remote(
             mod_tp.at[peer], mod_tp.at[peer], modt_send.at[k], modt_recv.at[peer], me_s, peer
         ).wait_recv()
-    copies[8].wait()
-    gather_start(w_out, wo_send, wo_recv)
 
     def vec(r):
         return jnp.concatenate([mod_tp[j][r : r + 1, :] for j in range(n_tp)], axis=1)
@@ -501,6 +523,7 @@
     k_trade.wait_recv()
     v_trade.wait_recv()
     halo_start(False)
+    gather_forward(wo_view(0), wo_sems(0))
     q_trade.wait_recv()
 
     for index, block_ctx in enumerate((ctx_k, ctx_v)):
@@ -569,12 +592,18 @@
     back_in = remote(
         att_slab, att.at[me_t, 1 - side], pair_send.at[3], pair_recv.at[3], mate, me_t
     )
+    first, second = att_view(side), att_view(1 - side)
+    gather_start(first, att_sems(0))
     back_in.wait_recv()
-    gather_forward(w_out, wo_send, wo_recv)
-    gather_start(att, att_send, att_recv)
-    gather_forward(att, att_send, att_recv)
-    gather_finish(w_out, wo_send, wo_recv)
-    gather_finish(att, att_send, att_recv)
+    gather_start(second, att_sems(1))
+    gather_forward(first, att_sems(0))
+    gather_forward(wo_view(1), wo_sems(1))
+    gather_forward(second, att_sems(1))
+    copies[8].wait()
+    gather_finish(wo_view(0), wo_sems(0))
+    gather_finish(wo_view(1), wo_sems(1))
+    gather_finish(first, att_sems(0))
+    gather_finish(second, att_sems(1))
     gate = vec(4)
     cols = 512
     for n in range(d // cols):
@@ -672,10 +701,10 @@
             dma((2, 2)),
             dma((2, n_sp)),
             dma((2, n_sp)),
-            dma((n_tp,)),
-            dma((n_tp,)),
-            dma((n_tp,)),
-            dma((n_tp,)),
+            dma((2, n_tp)),
+            dma((2, n_tp)),
+            dma((2, n_tp)),
+            dma((2, n_tp)),
         ],
         compiler_params=pltpu.CompilerParams(collective_id=0, has_side_effects=True),
         name="fused_block",

time: 50.1 us -> 45.2 us (0.902)
  Pallas kernels: 46.1 us -> 41.2 us
    pallas_call x1, Pallas kernels: 46.1 us -> 41.2 us  [per_device(): pl.pallas_call(functools.partial(fused_kernel, n_sp, n_tp), out_shape=jax...]
where the time goes in v3:
time: 45.2 us; the launch traced here: 44.9 us
  Pallas kernels  41.2 us (91%)
  local copies, waits for them, and re-layouts  3.67 us (8%)
    pallas_call x1, Pallas kernels, per_device(): pl.pallas_call(functools.partial(fused_kernel, n_sp, n_tp), out_shape=jax...  41.2 us
    unnamed x2, local copies, waits for them, and re-layouts  3.67 us

profile of v3, /device:TPU:1, one launch (start us, length us, event | category | flops | bytes accessed | tf_op | source)
XLA Modules:
  0.0 44.9 jit_solution(6529034088216226453)
XLA Ops:
  0.0 1.4 %copy.16.bias_in = f32[4,15,31]{2,1,0:T(8,128)} copy(f32[4,15,31]{2,0,1:T(4,128)} %param.28) | data formatting | bytes 14880 | tf_op args[13]
  1.4 41.2 %fused_block.1 = bf16[256,2048]{1,0:T(8,128)(2,1)} custom-call(bf16[256,2048]{1,0:T(8,128)(2,1)} %latent.1, bf16[64,2048]{1,0:T(8,128)(2,1)} %context.1, bf16[256,512]{1,0:T(8,128)(2,1)} %shift_w.1, bf16[256,512]{1,0:T(8,128)(2,1)} %scale_w.1, bf16[256,512]{1,0:T(8,128)(2,1)} %gate_w.1, bf16[2048,256]{1,0:T(8,128)(2,1)} %query_w.1, bf16[2048,256]{1,0:T(8,128)(2,1)} %key_w.1, ...), custom_call_target="tpu_custom_call" | custom-call | tf_op jit(solution)/shard_map/fused_block/pallas_call | solution.py:664
  42.6 2.3 %copy.18 = bf16[256,2048]{1,0:T(8,128)(2,1)} copy(bf16[256,2048]{1,0:T(8,128)(2,1)} %fused_block.1) | data formatting | bytes 2097152

commit v4 on v3

--- a/solution.py
+++ b/solution.py
@@ -386,7 +386,7 @@
     n_pairs = 2 * WIN_ROWS - 2
     bias_pad[...] = jnp.zeros_like(bias_pad)
     for h in range(heads):
-        bias_pad[h, : 2 * WIN_ROWS - 1, : 2 * WIN_COLS - 1] = bias_in[h]
+        bias_pad[h, : 2 * WIN_ROWS - 1, : 2 * WIN_COLS - 1] = bias_in[:, h, :]
     for h in range(half_heads):
         head = side * half_heads + h
         upper = pltpu.roll(bias_pad[head, 1 : n_pairs + 1, :], GRID_W, 1)
@@ -663,7 +663,7 @@
     dma = pltpu.SemaphoreType.DMA
     return pl.pallas_call(
         functools.partial(fused_kernel, n_sp, n_tp),
-        out_shape=jax.ShapeDtypeStruct((rows, d), BF16),
+        out_shape=pltpu.VMEM((rows, d), BF16),
         in_specs=[any_spec] * 9 + [vmem_spec] * 6,
         out_specs=vmem_spec,
         scratch_shapes=[
@@ -723,7 +723,7 @@
         norm_gain.reshape(1, -1),
         query_gain.reshape(1, -1),
         key_gain.reshape(1, -1),
-        offset_bias,
+        offset_bias.transpose(1, 0, 2),
     )
 
 

time: 45.2 us -> 41.4 us (0.916)
  local copies, waits for them, and re-layouts: 3.67 us -> 0.97 us
  Pallas kernels: 41.2 us -> 40.2 us
    unnamed x2 -> x1, local copies, waits for them, and re-layouts: 3.67 us -> 0.97 us
    pallas_call x1, Pallas kernels: 41.2 us -> 40.2 us  [per_device(): pl.pallas_call(functools.partial(fused_kernel, n_sp, n_tp), out_shape=plt...]
where the time goes in v4:
time: 41.4 us; the launch traced here: 41.2 us
  Pallas kernels  40.2 us (97%)
  local copies, waits for them, and re-layouts  0.97 us (2%)
    pallas_call x1, Pallas kernels, per_device(): pl.pallas_call(functools.partial(fused_kernel, n_sp, n_tp), out_shape=plt...  40.2 us
    unnamed x1, local copies, waits for them, and re-layouts  0.97 us

profile of v4, /device:TPU:1, one launch (start us, length us, event | category | flops | bytes accessed | tf_op | source)
XLA Modules:
  0.0 41.2 jit_solution(820660752048515153)
XLA Ops:
  0.0 40.2 %fused_block.1 = bf16[256,2048]{1,0:T(8,128)(2,1)S(1)} custom-call(bf16[256,2048]{1,0:T(8,128)(2,1)} %latent.1, bf16[64,2048]{1,0:T(8,128)(2,1)} %context.1, bf16[256,512]{1,0:T(8,128)(2,1)} %shift_w.1, bf16[256,512]{1,0:T(8,128)(2,1)} %scale_w.1, bf16[256,512]{1,0:T(8,128)(2,1)} %gate_w.1, bf16[2048,256]{1,0:T(8,128)(2,1)} %query_w.1, ...), custom_call_target="tpu_custom_call" | custom-call | tf_op jit(solution)/shard_map/fused_block/pallas_call | solution.py:664
  40.2 1.0 %copy.17 = bf16[256,2048]{1,0:T(8,128)(2,1)} copy(bf16[256,2048]{1,0:T(8,128)(2,1)S(1)} %fused_block.1) | data formatting | bytes 2097152

commit v5 on v4

--- a/solution.py
+++ b/solution.py
@@ -484,33 +484,33 @@
         )
         return down, up
 
-    def halo_start(mine):
-        for index, block_all in enumerate((k_all, v_all)):
-            down, up = halo_copies(index, block_all)
-            is_low = side == 0 if mine else side == 1
-
-            @pl.when(is_low & (slab > 0))
-            def _():
-                down.start()
-
-            @pl.when(jnp.logical_not(is_low) & (slab < last_slab))
-            def _():
-                up.start()
+    def halo_start(mine, index, block_all):
+        down, up = halo_copies(index, block_all)
+        is_low = side == 0 if mine else side == 1
+
+        @pl.when(is_low & (slab > 0))
+        def _():
+            down.start()
+
+        @pl.when(jnp.logical_not(is_low) & (slab < last_slab))
+        def _():
+            up.start()
 
     copies[5].wait()
     keys = head_scale(jnp.dot(hid[...], w_qkv[0], preferred_element_type=F32), key_gain)
     split(k_stage, keys[c_rows:])
     k_trade = trade(0, k_stage, k_all, own)
+    k_all[own, :] = k_stage[side]
+    halo_start(True, 0, k_all)
     split(ck_stage, keys[:c_rows])
-    k_all[own, :] = k_stage[side]
+    share_ctx(0, ck_stage, ctx_k)
     copies[6].wait()
     values = jnp.dot(hid[...], w_qkv[1], preferred_element_type=F32).astype(BF16)
     split(v_stage, values[c_rows:])
     v_trade = trade(1, v_stage, v_all, own)
+    v_all[own, :] = v_stage[side]
+    halo_start(True, 1, v_all)
     split(cv_stage, values[:c_rows])
-    v_all[own, :] = v_stage[side]
-    halo_start(True)
-    share_ctx(0, ck_stage, ctx_k)
     share_ctx(1, cv_stage, ctx_v)
     copies[7].wait()
     queries = head_scale(
@@ -521,8 +521,9 @@
     q_trade = trade(2, q_stage, q_all, q_own)
     q_all[q_own, :] = q_stage[side]
     k_trade.wait_recv()
+    halo_start(False, 0, k_all)
     v_trade.wait_recv()
-    halo_start(False)
+    halo_start(False, 1, v_all)
     gather_forward(wo_view(0), wo_sems(0))
     q_trade.wait_recv()
 

time: 41.4 us -> 40.6 us (0.981)
  Pallas kernels: 40.2 us -> 39.4 us
    pallas_call x1, Pallas kernels: 40.2 us -> 39.4 us  [per_device(): pl.pallas_call(functools.partial(fused_kernel, n_sp, n_tp), out_shape=plt...]
where the time goes in v5:
time: 40.6 us; the launch traced here: 40.4 us
  Pallas kernels  39.4 us (97%)
  local copies, waits for them, and re-layouts  0.97 us (2%)
    pallas_call x1, Pallas kernels, per_device(): pl.pallas_call(functools.partial(fused_kernel, n_sp, n_tp), out_shape=plt...  39.4 us
    unnamed x1, local copies, waits for them, and re-layouts  0.97 us

profile of v5, /device:TPU:1, one launch (start us, length us, event | category | flops | bytes accessed | tf_op | source)
XLA Modules:
  0.0 40.4 jit_solution(16294485750186569423)
XLA Ops:
  0.0 39.4 %fused_block.1 = bf16[256,2048]{1,0:T(8,128)(2,1)S(1)} custom-call(bf16[256,2048]{1,0:T(8,128)(2,1)} %latent.1, bf16[64,2048]{1,0:T(8,128)(2,1)} %context.1, bf16[256,512]{1,0:T(8,128)(2,1)} %shift_w.1, bf16[256,512]{1,0:T(8,128)(2,1)} %scale_w.1, bf16[256,512]{1,0:T(8,128)(2,1)} %gate_w.1, bf16[2048,256]{1,0:T(8,128)(2,1)} %query_w.1, ...), custom_call_target="tpu_custom_call" | custom-call | tf_op jit(solution)/shard_map/fused_block/pallas_call | solution.py:665
  39.4 1.0 %copy.17 = bf16[256,2048]{1,0:T(8,128)(2,1)} copy(bf16[256,2048]{1,0:T(8,128)(2,1)S(1)} %fused_block.1) | data formatting | bytes 2097152

commit v6 on v5

--- a/solution.py
+++ b/solution.py
@@ -346,7 +346,8 @@
             ).wait_recv()
 
     early = width // 4
-    wo_rows = (pl.ds(0, early), pl.ds(early, width - early))
+    later = (width - early) // 2
+    wo_rows = (pl.ds(0, early), pl.ds(early, later), pl.ds(early + later, later))
 
     def wo_view(c):
         return lambda j: w_out.at[j, wo_rows[c]]
@@ -414,6 +415,7 @@
         sends.append(c)
 
     gather_start(wo_view(1), wo_sems(1), wo_source(1))
+    gather_start(wo_view(2), wo_sems(2), wo_source(2))
 
     for k in range(1, n_tp):
         peer = lax.rem(me_t + k, n_tp)
@@ -587,6 +589,7 @@
     )
     back.start()
     sends.append(back)
+    gather_forward(wo_view(1), wo_sems(1))
     for i in range(l_rows):
         att[me_t, side, i * GRID_W : (i + 1) * GRID_W, :] = attend(side * l_rows + i)
 
@@ -598,11 +601,12 @@
     back_in.wait_recv()
     gather_start(second, att_sems(1))
     gather_forward(first, att_sems(0))
-    gather_forward(wo_view(1), wo_sems(1))
+    gather_forward(wo_view(2), wo_sems(2))
     gather_forward(second, att_sems(1))
     copies[8].wait()
     gather_finish(wo_view(0), wo_sems(0))
     gather_finish(wo_view(1), wo_sems(1))
+    gather_finish(wo_view(2), wo_sems(2))
     gather_finish(first, att_sems(0))
     gather_finish(second, att_sems(1))
     gate = vec(4)
@@ -702,8 +706,8 @@
             dma((2, 2)),
             dma((2, n_sp)),
             dma((2, n_sp)),
-            dma((2, n_tp)),
-            dma((2, n_tp)),
+            dma((3, n_tp)),
+            dma((3, n_tp)),
             dma((2, n_tp)),
             dma((2, n_tp)),
         ],

time: 40.6 us -> 40.7 us (level)
  no operation moved by 1% of the time
where the time goes in v6:
time: 40.7 us; the launch traced here: 40.4 us
  Pallas kernels  39.5 us (97%)
  local copies, waits for them, and re-layouts  0.97 us (2%)
    pallas_call x1, Pallas kernels, per_device(): pl.pallas_call(functools.partial(fused_kernel, n_sp, n_tp), out_shape=plt...  39.5 us
    unnamed x1, local copies, waits for them, and re-layouts  0.97 us

profile of v6, /device:TPU:1, one launch (start us, length us, event | category | flops | bytes accessed | tf_op | source)
XLA Modules:
  0.0 40.4 jit_solution(17685875617879833535)
XLA Ops:
  0.0 39.5 %fused_block.1 = bf16[256,2048]{1,0:T(8,128)(2,1)S(1)} custom-call(bf16[256,2048]{1,0:T(8,128)(2,1)} %latent.1, bf16[64,2048]{1,0:T(8,128)(2,1)} %context.1, bf16[256,512]{1,0:T(8,128)(2,1)} %shift_w.1, bf16[256,512]{1,0:T(8,128)(2,1)} %scale_w.1, bf16[256,512]{1,0:T(8,128)(2,1)} %gate_w.1, bf16[2048,256]{1,0:T(8,128)(2,1)} %query_w.1, ...), custom_call_target="tpu_custom_call" | custom-call | tf_op jit(solution)/shard_map/fused_block/pallas_call | solution.py:669
  39.5 1.0 %copy.17 = bf16[256,2048]{1,0:T(8,128)(2,1)} copy(bf16[256,2048]{1,0:T(8,128)(2,1)S(1)} %fused_block.1) | data formatting | bytes 2097152
